TPU v7x, 256 devices: a 4x2x16 block of a 4x16x16 slice. The times are simulated.
256 devices in a mesh: grp: 2 (over y), sp: 32 (over z, core), tp: 4 (over x).
Axes of the slice: x: 4, y: 2, z: 16, core: 2. Of those that a mesh axis runs over, the one named last changes fastest.
The devices are a block of a 4x16x16 slice.
Arguments:
- queries: bfloat16 [16384, 2048], P(('grp', 'sp'), 'tp'), parts along dimension 0, may hold values from -6 to 6
- keys: bfloat16 [16384, 2048], P(('grp', 'sp'), 'tp'), parts along dimension 0, may hold values from -6 to 6
- values: bfloat16 [16384, 2048], P(('grp', 'sp'), 'tp'), parts along dimension 0, may hold values from -8 to 8
- offsets: float32 [16], P('tp'), as said below
- residual: bfloat16 [16384, 4096], P(('grp', 'sp', 'tp')), parts along dimension 0, may hold values from -6 to 6
- out_weight: bfloat16 [2048, 4096], P('tp'), may hold values from -0.52734375 to 0.52734375
- gain_one: float32 [4096], replicated, may hold values from 0.1 to 1.9
- shift_one: float32 [4096], replicated, may hold values from -3 to 3
- gain_two: float32 [4096], replicated, may hold values from 0.1 to 1.9
- shift_two: float32 [4096], replicated, may hold values from -3 to 3
- group_prob: float32 [16384], P(('grp', 'sp', 'tp')), parts along dimension 0, may hold values from 0.2 to 1
- pair_logits: float32 [16384, 2], P(('grp', 'sp', 'tp')), parts along dimension 0, may hold values from -6 to 6
- routes: int32 [16384, 2], P(('grp', 'sp', 'tp')), parts along dimension 0, may hold values from 0 to 127, as said below
- w_gate: bfloat16 [128, 4096, 256], P(('sp', 'tp')), may hold values from -0.09375 to 0.09375
- w_up: bfloat16 [128, 4096, 256], P(('sp', 'tp')), may hold values from -0.09375 to 0.09375
- w_down: bfloat16 [128, 256, 4096], P(('sp', 'tp')), may hold values from -1.5 to 1.5
Outputs:
- layer_out: bfloat16 [16384, 4096], P(('grp', 'sp', 'tp')), parts along dimension 0
There are 2 independent parts, one for each index of `grp`. A program takes and returns all parts, laid end to end along the dimension named above; an argument that names none is the same for every part. Nothing has to cross between parts.
Inputs may be any that keep to these rules, and one draw needn't show every extreme that they name: `routes`: both experts of a token are different and lie in one group of 32 consecutive experts. Of the tokens of one device (64 consecutive ones), at most 2 name any one expert; in every draw some experts are named exactly 2 times by the tokens of every device. `offsets`: each offset lies between 2.5 and ln(8192) - 0.3.
All inputs are finite; a program needn't handle non-finite values.
Results may differ from a plain program's by a relative error of at most 0.014.
Values may be sent and summed in bfloat16 or wider, within the bound.
No kernel may reach another device: no remote copies, remote signals or barrier semaphores. Data moves between devices by JAX's collectives and lax.ppermute only.
A program may use at most 128 MiB of HBM per device.

v0:
```python
import math

import jax
import jax.numpy as jnp
from jax import lax
from jax.sharding import PartitionSpec as P

HEAD_DIM = 128
GROUPS = 4
TOPK = 2


residual_scale = 8.0**0.25
norm_eps = 1e-05


def sent_together(arrays, axis, dim, along):
    ends, at = ([], 0)
    for a in arrays[:-1]:
        at += a.shape[along]
        ends.append(at)
    both = jnp.concatenate(arrays, axis=along)
    return tuple(jnp.split(lax.all_gather(both, axis, axis=dim, tiled=True), ends, axis=along))


def cut_along(value, dim, peers):
    before, after = (value.shape[:dim], value.shape[dim + 1 :])
    return jnp.moveaxis(value.reshape(*before, peers, -1, *after), dim, 0)


def sent_and_summed(value, axis, dim):
    peers = lax.axis_size(axis)
    tiles = lax.all_to_all(cut_along(value, dim, peers), axis, 0, 0, tiled=True)
    return jnp.sum(tiles.astype(jnp.float32), axis=0)


def layer_norm(rows, gain, shift):
    mean = jnp.mean(rows, axis=-1, keepdims=True)
    centred = rows - mean
    variance = jnp.mean(centred * centred, axis=-1, keepdims=True)
    return centred * lax.rsqrt(variance + norm_eps) * gain + shift


def slot_index(routes, expert_count, capacity):
    flat = routes.reshape(-1)
    onehot = (flat[:, None] == jnp.arange(expert_count, dtype=jnp.int32)[None, :]).astype(jnp.int32)
    earlier = jnp.cumsum(onehot, axis=0) - onehot
    rank = jnp.sum(earlier * onehot, axis=1)
    return flat * capacity + rank


def expert_rows(rows, gate_w, up_w, down_w):
    gate = jnp.dot(rows, gate_w, preferred_element_type=jnp.float32)
    upper = jnp.dot(rows, up_w, preferred_element_type=jnp.float32)
    hidden = (jax.nn.silu(gate) * upper).astype(jnp.bfloat16)
    return jnp.dot(hidden, down_w, preferred_element_type=jnp.float32).astype(jnp.bfloat16)


def per_device(
    queries,
    keys,
    values,
    offsets,
    residual,
    out_weight,
    gain_one,
    shift_one,
    gain_two,
    shift_two,
    group_prob,
    pair_logits,
    routes,
    w_gate,
    w_up,
    w_down,
):
    row_count = queries.shape[0]
    head_count = offsets.shape[0]
    block_count = lax.axis_size("sp")
    own_start = lax.axis_index("sp") * row_count
    query_pos = own_start + jnp.arange(row_count, dtype=jnp.int32)
    last_query = jnp.max(query_pos)
    query_heads = queries.reshape(row_count, head_count, HEAD_DIM)
    score_scale = HEAD_DIM ** (-0.5)

    def scores(piece, start):
        key_heads = piece.reshape(piece.shape[0], head_count, HEAD_DIM)
        score = (
            jnp.einsum("qhd,khd->hqk", query_heads, key_heads, preferred_element_type=jnp.float32)
            * score_scale
            - offsets[:, None, None]
        )
        key_pos = start + jnp.arange(piece.shape[0], dtype=jnp.int32)
        strict = key_pos[None, :] < query_pos[:, None]
        keep = jnp.where(strict, jax.nn.log_sigmoid(-score), 0.0)
        return (score, strict, keep)

    def add_totals(totals, piece, start):

        def compute(current):
            score, strict, keep = scores(piece, start)
            count = piece.shape[0] // row_count
            sums = jnp.sum(keep.reshape(head_count, row_count, count, row_count), axis=3)
            first = start // row_count
            old = lax.dynamic_slice_in_dim(current, first, count, 2)
            return lax.dynamic_update_slice_in_dim(current, old + sums, first, 2)

        return lax.cond(start < last_query, compute, lambda current: current, totals)

    def value_adder(prefix, total):

        def add_values(acc, pieces, start):
            key_piece, value_piece = pieces

            def compute(current):
                score, strict, keep = scores(key_piece, start)
                base = lax.dynamic_slice_in_dim(prefix, start // row_count, 1, 2)
                later = total[:, :, None] - base - jnp.cumsum(keep, axis=2)
                weight = jnp.where(strict, jnp.exp(jax.nn.log_sigmoid(score) + later), 0.0).astype(
                    jnp.bfloat16
                )
                value_heads = value_piece.reshape(value_piece.shape[0], head_count, HEAD_DIM)
                return current + jnp.einsum(
                    "hqk,khd->qhd", weight, value_heads, preferred_element_type=jnp.float32
                )

            return lax.cond(start < last_query, compute, lambda current: current, acc)

        return add_values

    empty_totals = jnp.zeros((head_count, row_count, block_count), jnp.float32)
    empty_out = jnp.zeros((row_count, head_count, HEAD_DIM), jnp.float32)
    every_key, every_value = sent_together((keys, values), "sp", 0, 1)
    per_turn = math.gcd(block_count, max(1, 2048 // row_count))
    span_rows = per_turn * row_count

    def run_local(fold, init, operands, single):

        def step(turn, carry):
            start = (turn * span_rows).astype(jnp.int32)
            pieces = tuple(
                (lax.dynamic_slice_in_dim(operand, start, span_rows, 0) for operand in operands)
            )
            return fold(carry, pieces[0] if single else pieces, start)

        return lax.fori_loop(0, block_count // per_turn, step, init)

    totals = run_local(add_totals, empty_totals, (every_key,), True)
    prefix = jnp.cumsum(totals, axis=2) - totals
    total = jnp.sum(totals, axis=2)
    attended = run_local(value_adder(prefix, total), empty_out, (every_key, every_value), False)
    attended_rows = attended.reshape(row_count, head_count * HEAD_DIM).astype(jnp.bfloat16)
    local_rows = residual.shape[0]
    mixed = sent_and_summed(
        jnp.dot(attended_rows, out_weight, preferred_element_type=jnp.float32).astype(jnp.bfloat16),
        "tp",
        0,
    )
    normed = layer_norm(
        residual_scale * residual.astype(jnp.float32) + mixed, gain_one, shift_one
    ).astype(jnp.bfloat16)
    width = normed.shape[1]
    expert_count = lax.axis_size("sp") * lax.axis_size("tp")
    capacity = local_rows // (expert_count // GROUPS)
    slots = slot_index(routes, expert_count, capacity)
    buffer = (
        jnp.zeros((expert_count * capacity, width), jnp.bfloat16)
        .at[slots]
        .set(jnp.repeat(normed, TOPK, axis=0))
    )
    arrived = lax.all_to_all(
        buffer.reshape(expert_count, capacity, width),
        ("sp", "tp"),
        split_axis=0,
        concat_axis=0,
        tiled=True,
    )
    result = expert_rows(arrived.reshape(-1, width), w_gate[0], w_up[0], w_down[0]).reshape(
        expert_count, capacity, width
    )
    returned = lax.all_to_all(result, ("sp", "tp"), split_axis=0, concat_axis=0, tiled=True)
    picked = returned.reshape(-1, width)[slots].reshape(local_rows, TOPK, width)
    difference = pair_logits[:, 0] - pair_logits[:, 1]
    pair_weight = jnp.stack([jax.nn.sigmoid(difference), jax.nn.sigmoid(-difference)], axis=1)
    route_weight = group_prob[:, None] * pair_weight
    moe = jnp.sum(route_weight[:, :, None] * picked.astype(jnp.float32), axis=1)
    return layer_norm(
        residual_scale * normed.astype(jnp.float32) + moe, gain_two, shift_two
    ).astype(jnp.bfloat16)


def solution(mesh):
    return jax.shard_map(
        per_device,
        mesh=mesh,
        in_specs=(
            P(("grp", "sp"), "tp"),
            P(("grp", "sp"), "tp"),
            P(("grp", "sp"), "tp"),
            P("tp"),
            P(("grp", "sp", "tp"), None),
            P("tp", None),
            P(),
            P(),
            P(),
            P(),
            P(("grp", "sp", "tp")),
            P(("grp", "sp", "tp"), None),
            P(("grp", "sp", "tp"), None),
            P(("sp", "tp"), None, None),
            P(("sp", "tp"), None, None),
            P(("sp", "tp"), None, None),
        ),
        out_specs=P(("grp", "sp", "tp"), None),
        check_vma=False,
    )
```

profile of v0, /device:TPU:33, one launch (start us, length us, event | category | flops | bytes accessed | tf_op | source)
XLA Modules:
  0.0 749.1 jit_solution(11493425176619980592)
XLA Ops:
  12.4 140.7 %all-gather.2.cloned.1.call-done = bf16[8192,1024]{0,1:T(8,128)(2,1)} async-done(((bf16[256,1024]{0,1:T(8,128)(2,1)}), bf16[8192,1024]{0,1:T(8,128)(2,1)}) %all-gather.2.cloned.1.call-update) | async-done | bytes 16777232 | tf_op jit(solution)/shard_map/all_gather | solution.py:23
  153.1 11.6 %fusion.51 = (bf16[8192,512]{0,1:T(8,128)(2,1)}, bf16[8192,512]{0,1:T(8,128)(2,1)}) fusion(bf16[8192,1024]{0,1:T(8,128)(2,1)} %all-gather.2.cloned.1.call-done), kind=kLoop, calls=%fused_computation.96 | loop fusion | bytes 33554432 | tf_op jit(solution)/shard_map/split | solution.py:23
  164.7 13.0 %while.34 = (s32[]{:T(128)}, f32[4,256,32]{1,2,0:T(8,128)S(1)}, s32[]{:T(128)}, bf16[8192,512]{0,1:T(8,128)(2,1)}, bf16[256,4,128]{2,0,1:T(8,128)(2,1)}, /*index=5*/f32[4]{0:T(128)S(1)}, s32[]{:T(128)}, s32[]{:T(128)}, s32[]{:T(128)}) while((s32[]{:T(128)}, f32[4,256,32]{1,2,0:T(8,128)S(1)}, s32[]{:T(128)}, ...), condition=%wide.region_5.6_spmd.clone, body=%wide.region_1.5_spmd.clone.sunk | while | flops 560466176 | bytes 7819692 | solution.py:146
  165.3 10.3 %conditional.6 = (f32[4,256,32]{1,2,0:T(8,128)S(1)}) conditional(s32[]{:T(128)} %convert_element_type.103, f32[4,256,32]{1,2,0:T(8,128)S(1)} %get-tuple-element.735, (s32[]{:T(128)}, f32[4,256,32]{1,2,0:T(8,128)S(1)}, s32[]{:T(128)}, bf16[8192,512]{0,1:T(8,128)(2,1)}, bf16[256,4,128]{2,0,1:T(8,128)(2,1)}, /*index=5*/f32[4]{0:T(128)S(1)}, ...), branch_computations={%region_2.0_spmd, %region_3.4_spmd} | conditional | flops 560466176 | bytes 7818493 | solution.py:108
  167.6 7.8 %bitcast_reduce_fusion = f32[4,256,8]{1,2,0:T(8,128)S(1)} fusion(bf16[2048,4,128]{0,2,1:T(8,128)(2,1)S(1)} %bitcast.95, bf16[256,4,128]{2,0,1:T(8,128)(2,1)} %get-tuple-element.453, f32[4]{0:T(128)S(1)} %get-tuple-element.454, pred[256,2048]{0,1:T(8,128)(4,1)S(1)} %broadcast_compare_fusion), kind=kOutput, calls=%fused_computation.7 | convolution fusion | flops 559931392 | bytes 2916368 | tf_op jit(solution)/shard_map/while/body/eval_jaxpr/cond/branch_1_fun/qhd,khd->hqk/dot_general | solution.py:89
  178.0 70.3 %while.35 = (s32[]{:T(128)}, f32[256,4,128]{2,0,1:T(8,128)S(1)}, s32[]{:T(128)}, bf16[8192,512]{0,1:T(8,128)(2,1)}, bf16[256,4,128]{2,0,1:T(8,128)(2,1)}, /*inde...) while((s32[]{:T(128)}, f32[256,4,128]{2,0,1:T(8,128)S(1)}, ...), condition=%wide.region_13.14_spmd.clone, body=%wide.region_8.13_spmd.clone.sunk | while | flops 1393428736 | bytes 116630016 | solution.py:146
  193.0 52.8 %conditional.7 = (f32[256,4,128]{2,0,1:T(8,128)S(1)}) conditional(s32[]{:T(128)} %convert_element_type.104, f32[256,4,128]{2,0,1:T(8,128)S(1)} %get-tuple-element.765, (s32[]{:T(128)}, s32[]{:T(128)}, bf16[8192,512]{0,1:T(8,128)(2,1)}, bf16[256,4,128]{2,0,1:T(8,128)(2,1)}, f32[4]{0:T(128)S(1)}, /*index=5*/f32[4,256]{1,0:T(4,128)S(1)}, ...), branch_computations={%region_9.9_spmd, %region_10.12_spmd} | conditional | flops 1393428736 | bytes 116628768 | solution.py:127
  193.0 4.2 constant_dynamic-slice_fusion.1
  197.7 10.7 %fusion.16 = (f32[4,256,2048]{1,2,0:T(8,128)}, f32[4,2048,256]{2,1,0:T(8,128)}) fusion(f32[4]{0:T(128)S(1)} %get-tuple-element.468, pred[256,2048]{0,1:T(8,128)(4,1)S(1)} %broadcast_compare_fusion.1, bf16[2048,4,128]{0,2,1:T(8,128)(2,1)S(1)} %bitcast.96, bf16[256,4,128]{2,0,1:T(8,128)(2,1)} %get-tuple-element.467), kind=kOutput, calls=%fused_computation.27 | convolution fusion | flops 557842432 | bytes 19660816 | tf_op jit(solution)/shard_map/while/body/eval_jaxpr/cond/branch_1_fun/qhd,khd->hqk/dot_general | solution.py:89
  208.3 11.4 %fusion.21 = f32[4,256,16,128]{1,2,3,0:T(8,128)} fusion(f32[4,256,16,128]{1,3,2,0:T(8,128)} %bitcast.93), kind=kOutput, calls=%fused_computation.36 | output fusion | flops 266338304 | bytes 16777216 | tf_op jit(solution)/shard_map/reduce-window.6
  220.7 4.4 broadcast_add_fusion.1
  225.2 8.1 %copy.47 = f32[4,256,16,128]{1,3,2,0:T(8,128)} copy(f32[4,256,16,128]{1,2,3,0:T(8,128)S(1)} %broadcast_add_fusion.1) | data formatting | bytes 16777216 | tf_op jit(solution)/shard_map/reduce_window_sum
  233.2 10.9 %fusion.14 = bf16[4,256,2048]{1,2,0:T(8,128)(2,1)S(1)} fusion(f32[4,256,16,128]{1,3,2,0:T(8,128)} %copy.47, f32[4,2048,256]{2,1,0:T(8,128)} %get-tuple-element.612, f32[4,256]{1,0:T(4,128)S(1)} %fusion.24, f32[4]{0:T(128)S(1)} %get-tuple-element.468, pred[256,2048]{0,1:T(8,128)(4,1)S(1)} %broadcast_compare_fusion.1), kind=kLoop, calls=%fused_computation.25 | loop fusion | flops 29360128 | bytes 21499920 | tf_op jit(solution)/shard_map/while/body/eval_jaxpr/cond/branch_1_fun/convert_element_type | solution.py:119
  248.4 4.8 convolution_convert_fusion.1
  253.2 4.7 all-to-all-start
  258.8 25.2 %all-to-all-done = bf16[4,64,4096]{2,1,0:T(8,128)(2,1)} async-done(((bf16[4,64,4096]{2,1,0:T(8,128)(2,1)}), bf16[4,64,4096]{2,1,0:T(8,128)(2,1)}, u32[]{:S(2)}, u32[]{:S(2)}) %all-to-all-start) | async-done | bytes 2097184 | tf_op jit(solution)/shard_map/all_to_all | solution.py:33
  284.0 2.1 convert_reduce_fusion
  287.0 2.0 broadcast_in_dim.57
  289.1 2.3 reshape.190
  291.3 4.3 scatter_custom_fusion
  295.7 4.4 reshape.173
  300.1 297.3 %all_to_all.15 = bf16[128,2,4096]{2,1,0:T(2,128)(2,1)} all-to-all(bf16[128,2,4096]{2,1,0:T(2,128)(2,1)} %reshape.173), channel_id=1, replica_groups=mesh['grp'=2,'sp'=32,'tp'=4] {'sp','tp'}, dimensions={0} | all-to-all | bytes 4194304 | tf_op jit(solution)/shard_map/all_to_all | solution.py:171
  597.4 4.1 reshape.174
  601.5 2.9 fusion.28
  604.5 5.9 convolution_convert_fusion
  610.4 4.4 reshape.175
  614.9 10.5 %all-to-all-start.2 = ((bf16[128,2,4096]{2,1,0:T(2,128)(2,1)}), bf16[128,2,4096]{2,1,0:T(2,128)(2,1)}, u32[]{:S(2)}, u32[]{:S(2)}) async-start(bf16[128,2,4096]{2,1,0:T(2,128)(2,1)} %reshape.175), calls=%async_computation.2 | async-start | bytes 4194304 | tf_op jit(solution)/shard_map/all_to_all | solution.py:181
  625.5 97.4 %all-to-all-done.2 = bf16[128,2,4096]{2,1,0:T(2,128)(2,1)} async-done(((bf16[128,2,4096]{2,1,0:T(2,128)(2,1)}), bf16[128,2,4096]{2,1,0:T(2,128)(2,1)}, u32[]{:S(2)}, u32[]{:S(2)}) %all-to-all-start.2) | async-done | bytes 2097184 | tf_op jit(solution)/shard_map/all_to_all | solution.py:181
  722.9 4.1 reshape.176
  727.0 5.0 gather_fusion
  732.0 3.4 reshape.177
  735.5 4.8 multiply_reduce_fusion
  (87 shorter events, 15.4 us)
Async XLA Ops:
  6.5 597.9 %copy-start = (bf16[1,256,4096]{2,1,0:T(8,128)(2,1)S(1)}, bf16[1,256,4096]{2,1,0:T(8,128)(2,1)}, u32[]{:S(2)}) copy-start(bf16[1,256,4096]{2,1,0:T(8,128)(2,1)} %param.39) | copy-start | bytes 6291460
  6.6 146.6 %all-gather.2.cloned.1.call-start = ((), (), s32[]{:S(2)}) async-start(), calls=%async_computation.3 | async-start | bytes 17301504 | tf_op jit(solution)/shard_map/all_gather | solution.py:23
  12.4 152.3 %copy-start.7 = (f32[4]{0:T(128)S(1)}, f32[4]{0:T(128)}, u32[]{:S(2)}) copy-start(f32[4]{0:T(128)} %param.27) | copy-start | bytes 52
  233.2 11.0 %copy-start.1 = (bf16[2048,512]{0,1:T(8,128)(2,1)S(1)}, bf16[2048,512]{0,1:T(8,128)(2,1)}, u32[]{:S(2)}) copy-start(bf16[2048,512]{0,1:T(8,128)(2,1)} %get-tuple-element.613) | copy-start | bytes 6291460 | tf_op jit(solution)/shard_map/while/body/eval_jaxpr/cond
  248.4 9.4 %copy-start.8 = (s32[64,2]{0,1:T(2,128)S(1)}, s32[64,2]{0,1:T(2,128)}, u32[]{:S(2)}) copy-start(s32[64,2]{0,1:T(2,128)} %param.36) | copy-start | bytes 1540
  253.2 32.9 %copy-start.2 = (bf16[64,4096]{1,0:T(8,128)(2,1)S(1)}, bf16[64,4096]{1,0:T(8,128)(2,1)}, u32[]{:S(2)}) copy-start(bf16[64,4096]{1,0:T(8,128)(2,1)} %param.28) | copy-start | bytes 1572868
  253.2 30.8 %all-to-all-start = ((bf16[4,64,4096]{2,1,0:T(8,128)(2,1)}), bf16[4,64,4096]{2,1,0:T(8,128)(2,1)}, u32[]{:S(2)}, u32[]{:S(2)}) async-start(bf16[4,64,4096]{2,1,0:T(8,128)(2,1)} %bitcast.97), calls=%async_computation | async-start | bytes 4194304 | tf_op jit(solution)/shard_map/all_to_all | solution.py:33
  257.9 28.8 %copy-start.3 = (f32[4096]{0:T(1024)S(1)}, f32[4096]{0:T(1024)}, u32[]{:S(2)}) copy-start(f32[4096]{0:T(1024)} %param.31) | copy-start | bytes 49156
  257.9 28.8 %copy-start.4 = (f32[4096]{0:T(1024)S(1)}, f32[4096]{0:T(1024)}, u32[]{:S(2)}) copy-start(f32[4096]{0:T(1024)} %param.30) | copy-start | bytes 49156
  610.4 14.9 %copy-start.9 = (f32[64,2]{0,1:T(2,128)S(1)}, f32[64,2]{0,1:T(2,128)}, u32[]{:S(2)}) copy-start(f32[64,2]{0,1:T(2,128)} %param.35) | copy-start | bytes 1540
  610.4 14.9 %copy-start.10 = (f32[64]{0:T(128)S(1)}, f32[64]{0:T(128)}, u32[]{:S(2)}) copy-start(f32[64]{0:T(128)} %param.34) | copy-start | bytes 772
  614.9 108.0 %all-to-all-start.2 = ((bf16[128,2,4096]{2,1,0:T(2,128)(2,1)}), bf16[128,2,4096]{2,1,0:T(2,128)(2,1)}, u32[]{:S(2)}, u32[]{:S(2)}) async-start(bf16[128,2,4096]{2,1,0:T(2,128)(2,1)} %reshape.175), calls=%async_computation.2 | async-start | bytes 4194304 | tf_op jit(solution)/shard_map/all_to_all | solution.py:181
  732.0 8.8 %copy-start.5 = (f32[4096]{0:T(1024)S(1)}, f32[4096]{0:T(1024)}, u32[]{:S(2)}) copy-start(f32[4096]{0:T(1024)} %param.33) | copy-start | bytes 49156
  732.0 8.8 %copy-start.6 = (f32[4096]{0:T(1024)S(1)}, f32[4096]{0:T(1024)}, u32[]{:S(2)}) copy-start(f32[4096]{0:T(1024)} %param.32) | copy-start | bytes 49156
Sparse Core Ops, SparseCore 0:
  9.9 143.1 all-gather.1
where the time goes:
time: 748 us; the launch traced here: 749 us
  blocking collectives  297 us (40%)
  waiting for transfers between devices  263 us (35%)
  local copies, waits for them, and re-layouts  65.8 us (9%)
  other arithmetic  39.4 us (5%)
  matrix products  33.8 us (5%)
  loops' own time  20.3 us (3%)
  starting transfers between devices  15.1 us (2%)
  between operations  13.9 us (2%)
    all_to_all x1, blocking collectives, per_device(): lax.all_to_all(buffer.reshape(expert_count, capacity, width), ('sp', 'tp'...  297 us
    all_gather x1, waiting for transfers between devices, sent_together(): lax.all_gather(both, axis, axis=dim, tiled=True)  141 us
    all_to_all x1, waiting for transfers between devices, per_device(): lax.all_to_all(result, ('sp', 'tp'), split_axis=0, concat_axis=0, tiled=T...  97.4 us
    all_to_all x1, waiting for transfers between devices, sent_and_summed(): tiles = lax.all_to_all(cut_along(value, dim, peers), axis, 0, 0, tiled=True)  25.2 us
    another operation x2, loops' own time, run_local(): return lax.fori_loop(0, block_count // per_turn, step, init)  20.1 us
    dot_general x2, matrix products, scores(): jnp.einsum('qhd,khd->hqk', query_heads, key_heads, preferred_element_type...  18.5 us
    another operation x3, other arithmetic  15.9 us
  transfers between devices with their start and end apart: 3, of which 3 were waited for; matrix products, arithmetic and copies ran while one was open for 0% of the time, Pallas kernels for 0%

commit v1 on v0

v1 whole, which is shorter than its diff:
```python
import functools
import jax
import jax.numpy as jnp
from jax import lax
from jax.experimental import pallas as pl
from jax.experimental.pallas import tpu as pltpu
from jax.sharding import PartitionSpec as P

HEAD_DIM = 128
GROUPS = 4
TOPK = 2


residual_scale = 8.0**0.25
norm_eps = 1e-05


LOG2E = 1.4426950408889634
def attn_body(where_ref, off_ref, q_ref, kv_ref, o_ref, acc_ref, carry_ref, *, heads, span, per_step, lo):
    step = pl.program_id(0)
    own = where_ref[0]
    top_step = own // per_step
    rows = q_ref.shape[0]
    scale = HEAD_DIM ** (-0.5) * LOG2E
    from_s = lax.broadcasted_iota(jnp.int32, (span, span), 0)
    to_s = lax.broadcasted_iota(jnp.int32, (span, span), 1)
    later = (from_s >= to_s).astype(jnp.float32).astype(jnp.bfloat16)
    both = jnp.concatenate([later, later], axis=0) if lo else later
    shift = to_s - from_s

    def blocks(masked):
        first = own - top_step * per_step
        for h in range(heads):
            cols = slice(h * HEAD_DIM, (h + 1) * HEAD_DIM)
            q = q_ref[:, cols]
            carry = carry_ref[:, cols][:, :1]
            acc = acc_ref[:, cols]
            for b in reversed(range(per_step)):
                k = kv_ref[b * span:(b + 1) * span, 2 * h * HEAD_DIM:(2 * h + 1) * HEAD_DIM]
                v = kv_ref[b * span:(b + 1) * span, (2 * h + 1) * HEAD_DIM:(2 * h + 2) * HEAD_DIM]
                s = lax.dot_general(q, k, (((1,), (1,)), ((), ())), preferred_element_type=jnp.float32)
                y = s * scale - off_ref[h] * LOG2E
                soft = jnp.maximum(y, jnp.log(1.0 + jnp.exp2(jnp.minimum(y, 126.0))) * LOG2E)
                if masked:
                    strict = shift < (first - b) * span
                    soft = jnp.where(strict, soft, 0.0)
                high = soft.astype(jnp.bfloat16)
                if lo:
                    low = (soft - high.astype(jnp.float32)).astype(jnp.bfloat16)
                    high = jnp.concatenate([high, low], axis=1)
                sums = jnp.dot(high, both, preferred_element_type=jnp.float32)
                weight = jnp.exp2(y - carry - sums)
                if masked:
                    weight = jnp.where(strict, weight, 0.0)
                carry = carry + sums[:, :1]
                acc = acc + jnp.dot(weight.astype(jnp.bfloat16), v, preferred_element_type=jnp.float32)
            carry_ref[:, cols] = jnp.broadcast_to(carry, (rows, HEAD_DIM))
            acc_ref[:, cols] = acc

    @pl.when(step == 0)
    def _():
        acc_ref[...] = jnp.zeros_like(acc_ref)
        carry_ref[...] = jnp.zeros_like(carry_ref)
        blocks(True)

    @pl.when((step > 0) & (step <= top_step))
    def _():
        blocks(False)

    @pl.when(step == pl.num_programs(0) - 1)
    def _():
        o_ref[...] = acc_ref[...].astype(jnp.bfloat16)

def attend(own, offsets, q, kv, heads, per_step=4, lo=False):
    rows = q.shape[0]
    span = rows
    blocks = kv.shape[0] // span
    w = heads * HEAD_DIM
    body = functools.partial(attn_body, heads=heads, span=span, per_step=per_step, lo=lo)
    return pl.pallas_call(
        body,
        grid_spec=pltpu.PrefetchScalarGridSpec(
            num_scalar_prefetch=2,
            grid=(blocks // per_step,),
            in_specs=[pl.BlockSpec((rows, w), lambda n, at, off: (0, 0)),
                      pl.BlockSpec((per_step * span, 2 * w), lambda n, at, off: (jnp.maximum(at[0] // per_step - n, 0), 0))],
            out_specs=pl.BlockSpec((rows, w), lambda n, at, off: (0, 0)),
            scratch_shapes=[pltpu.VMEM((rows, w), jnp.float32), pltpu.VMEM((rows, w), jnp.float32)],
        ),
        out_shape=jax.ShapeDtypeStruct((rows, w), jnp.bfloat16),
        name="attend",
    )(own, offsets, q, kv)


def cut_along(value, dim, peers):
    before, after = (value.shape[:dim], value.shape[dim + 1 :])
    return jnp.moveaxis(value.reshape(*before, peers, -1, *after), dim, 0)


def sent_and_summed(value, axis, dim):
    peers = lax.axis_size(axis)
    tiles = lax.all_to_all(cut_along(value, dim, peers), axis, 0, 0, tiled=True)
    return jnp.sum(tiles.astype(jnp.float32), axis=0)


def layer_norm(rows, gain, shift):
    mean = jnp.mean(rows, axis=-1, keepdims=True)
    centred = rows - mean
    variance = jnp.mean(centred * centred, axis=-1, keepdims=True)
    return centred * lax.rsqrt(variance + norm_eps) * gain + shift


def slot_index(routes, expert_count, capacity):
    flat = routes.reshape(-1)
    onehot = (flat[:, None] == jnp.arange(expert_count, dtype=jnp.int32)[None, :]).astype(jnp.int32)
    earlier = jnp.cumsum(onehot, axis=0) - onehot
    rank = jnp.sum(earlier * onehot, axis=1)
    return flat * capacity + rank


def expert_rows(rows, gate_w, up_w, down_w):
    gate = jnp.dot(rows, gate_w, preferred_element_type=jnp.float32)
    upper = jnp.dot(rows, up_w, preferred_element_type=jnp.float32)
    hidden = (jax.nn.silu(gate) * upper).astype(jnp.bfloat16)
    return jnp.dot(hidden, down_w, preferred_element_type=jnp.float32).astype(jnp.bfloat16)


def per_device(
    queries,
    keys,
    values,
    offsets,
    residual,
    out_weight,
    gain_one,
    shift_one,
    gain_two,
    shift_two,
    group_prob,
    pair_logits,
    routes,
    w_gate,
    w_up,
    w_down,
):
    row_count = queries.shape[0]
    head_count = offsets.shape[0]
    own = lax.axis_index("sp").astype(jnp.int32).reshape(1)
    pairs = []
    for h in range(head_count):
        cols = slice(h * HEAD_DIM, (h + 1) * HEAD_DIM)
        pairs += [keys[:, cols], values[:, cols]]
    every = lax.all_gather(jnp.concatenate(pairs, axis=1), "sp", axis=0, tiled=True)
    attended_rows = attend(own, offsets, queries, every, head_count)
    local_rows = residual.shape[0]
    mixed = sent_and_summed(
        jnp.dot(attended_rows, out_weight, preferred_element_type=jnp.float32).astype(jnp.bfloat16),
        "tp",
        0,
    )
    normed = layer_norm(
        residual_scale * residual.astype(jnp.float32) + mixed, gain_one, shift_one
    ).astype(jnp.bfloat16)
    width = normed.shape[1]
    expert_count = lax.axis_size("sp") * lax.axis_size("tp")
    capacity = local_rows // (expert_count // GROUPS)
    slots = slot_index(routes, expert_count, capacity)
    buffer = (
        jnp.zeros((expert_count * capacity, width), jnp.bfloat16)
        .at[slots]
        .set(jnp.repeat(normed, TOPK, axis=0))
    )
    arrived = lax.all_to_all(
        buffer.reshape(expert_count, capacity, width),
        ("sp", "tp"),
        split_axis=0,
        concat_axis=0,
        tiled=True,
    )
    result = expert_rows(arrived.reshape(-1, width), w_gate[0], w_up[0], w_down[0]).reshape(
        expert_count, capacity, width
    )
    returned = lax.all_to_all(result, ("sp", "tp"), split_axis=0, concat_axis=0, tiled=True)
    picked = returned.reshape(-1, width)[slots].reshape(local_rows, TOPK, width)
    difference = pair_logits[:, 0] - pair_logits[:, 1]
    pair_weight = jnp.stack([jax.nn.sigmoid(difference), jax.nn.sigmoid(-difference)], axis=1)
    route_weight = group_prob[:, None] * pair_weight
    moe = jnp.sum(route_weight[:, :, None] * picked.astype(jnp.float32), axis=1)
    return layer_norm(
        residual_scale * normed.astype(jnp.float32) + moe, gain_two, shift_two
    ).astype(jnp.bfloat16)


def solution(mesh):
    return jax.shard_map(
        per_device,
        mesh=mesh,
        in_specs=(
            P(("grp", "sp"), "tp"),
            P(("grp", "sp"), "tp"),
            P(("grp", "sp"), "tp"),
            P("tp"),
            P(("grp", "sp", "tp"), None),
            P("tp", None),
            P(),
            P(),
            P(),
            P(),
            P(("grp", "sp", "tp")),
            P(("grp", "sp", "tp"), None),
            P(("grp", "sp", "tp"), None),
            P(("sp", "tp"), None, None),
            P(("sp", "tp"), None, None),
            P(("sp", "tp"), None, None),
        ),
        out_specs=P(("grp", "sp", "tp"), None),
        check_vma=False,
    )
```

time: 748 us -> 481 us (0.64)
  blocking collectives: 297 us -> 134 us
  other arithmetic: 39.4 us -> 9.89 us
  local copies, waits for them, and re-layouts: 65.8 us -> 42.7 us
  loops' own time: 20.3 us -> 0 us
  matrix products: 33.8 us -> 13.7 us
  waiting for transfers between devices: 263 us -> 243 us
  Pallas kernels: 0 us -> 7.54 us
    all_to_all x1, blocking collectives: 297 us -> 134 us  [per_device(): lax.all_to_all(buffer.reshape(expert_count, capacity, width), ('sp', 'tp'...]
    all_gather x1, waiting for transfers between devices: 141 us -> 120 us  [per_device(): lax.all_gather(jnp.concatenate(pairs, axis=1), 'sp', axis=0, tiled=True)]
    another operation x10 -> x0, loops' own time: 20.3 us -> none  [the longest x2 20.1 us: run_local(): return lax.fori_loop(0, block_count // per_turn, step, init)]
    dot_general x3 -> x0, matrix products: 20.1 us -> none  [the longest x2 18.5 us: scores(): jnp.einsum('qhd,khd->hqk', query_heads, key_heads, preferred_element_type...]
    another operation x4 -> x0, other arithmetic: 16.1 us -> none
    split x1 -> x0, local copies, waits for them, and re-layouts: 11.6 us -> none  [sent_together(): jnp.split(lax.all_gather(both, axis, axis=dim, tiled=True), ends, axis=al...]
    convert_element_type x1 -> x0, other arithmetic: 10.9 us -> none  [compute(): jnp.where(strict, jnp.exp(jax.nn.log_sigmoid(score) + later), 0.0)]
    another operation x3 -> x0, local copies, waits for them, and re-layouts: 8.92 us -> none
where the time goes in v1:
time: 481 us; the launch traced here: 480 us
  waiting for transfers between devices  243 us (51%)
  blocking collectives  134 us (28%)
  local copies, waits for them, and re-layouts  42.7 us (9%)
  starting transfers between devices  15.1 us (3%)
  matrix products  13.7 us (3%)
  between operations  13.7 us (3%)
  other arithmetic  9.89 us (2%)
  Pallas kernels  7.54 us (2%)
    all_to_all x1, blocking collectives, per_device(): lax.all_to_all(buffer.reshape(expert_count, capacity, width), ('sp', 'tp'...  134 us
    all_gather x1, waiting for transfers between devices, per_device(): lax.all_gather(jnp.concatenate(pairs, axis=1), 'sp', axis=0, tiled=True)  120 us
    all_to_all x1, waiting for transfers between devices, per_device(): lax.all_to_all(result, ('sp', 'tp'), split_axis=0, concat_axis=0, tiled=T...  97.7 us
    all_to_all x1, waiting for transfers between devices, sent_and_summed(): tiles = lax.all_to_all(cut_along(value, dim, peers), axis, 0, 0, tiled=True)  25 us
    all_to_all x1, starting transfers between devices, per_device(): lax.all_to_all(result, ('sp', 'tp'), split_axis=0, concat_axis=0, tiled=T...  10.2 us
  transfers between devices with their start and end apart: 3, of which 3 were waited for; matrix products, arithmetic and copies ran while one was open for 0% of the time, Pallas kernels for 0%

profile of v1, /device:TPU:33, one launch (start us, length us, event | category | flops | bytes accessed | tf_op | source)
XLA Modules:
  0.0 479.6 jit_solution(2613779955281226776)
XLA Ops:
  6.6 1.0 slice_dynamic-update-slice_fusion.7
  7.6 0.9 slice_dynamic-update-slice_fusion.6
  8.4 0.9 slice_dynamic-update-slice_fusion.5
  9.3 0.9 slice_dynamic-update-slice_fusion.4
  10.1 0.9 slice_dynamic-update-slice_fusion.3
  11.0 0.9 slice_dynamic-update-slice_fusion.2
  11.9 0.9 slice_dynamic-update-slice_fusion.1
  12.7 0.9 slice_dynamic-update-slice_fusion
  13.6 0.8 copy-done.2
  14.5 120.0 %all-gather.2.cloned.1.call-done.kv_ref = bf16[8192,1024]{1,0:T(8,128)(2,1)} async-done(((bf16[256,1024]{1,0:T(8,128)(2,1)}), bf16[8192,1024]{1,0:T(8,128)(2,1)}) %all-gather.2.cloned.1.call-update) | async-done | bytes 16777232 | tf_op jit(solution)/shard_map/all_gather | solution.py:153
  134.5 7.5 %attend.1 = bf16[256,512]{1,0:T(8,128)(2,1)} custom-call(s32[1]{0:T(128)} %bitcast.where_ref, f32[4]{0:T(128)} %off_ref.1, bf16[256,512]{1,0:T(8,128)(2,1)} %q_ref.1, bf16[8192,1024]{1,0:T(8,128)(2,1)} %all-gather.2.cloned.1.call-done.kv_ref), custom_call_target="tpu_custom_call" | custom-call | tf_op jit(solution)/shard_map/attend/pallas_call | solution.py:80
  142.0 4.8 %convolution_convert_fusion.1 = bf16[256,4096]{1,0:T(8,128)(2,1)} fusion(bf16[256,512]{1,0:T(8,128)(2,1)} %attend.1, bf16[512,4096]{1,0:T(8,128)(2,1)} %param.21), kind=kOutput, calls=%fused_computation.3 | convolution fusion | flops 1074790400 | bytes 6553600 | tf_op jit(solution)/shard_map/dot_general | solution.py:157
  146.8 4.8 %all-to-all-start = ((bf16[4,64,4096]{2,1,0:T(8,128)(2,1)}), bf16[4,64,4096]{2,1,0:T(8,128)(2,1)}, u32[]{:S(2)}, u32[]{:S(2)}) async-start(bf16[4,64,4096]{2,1,0:T(8,128)(2,1)} %bitcast.27), calls=%async_computation | async-start | bytes 4194304 | tf_op jit(solution)/shard_map/all_to_all | solution.py:102
  152.6 25.0 %all-to-all-done = bf16[4,64,4096]{2,1,0:T(8,128)(2,1)} async-done(((bf16[4,64,4096]{2,1,0:T(8,128)(2,1)}), bf16[4,64,4096]{2,1,0:T(8,128)(2,1)}, u32[]{:S(2)}, u32[]{:S(2)}) %all-to-all-start) | async-done | bytes 2097184 | tf_op jit(solution)/shard_map/all_to_all | solution.py:102
  177.7 2.1 convert_reduce_fusion
  180.8 2.0 broadcast_in_dim.5
  182.8 2.3 reshape.132
  185.1 4.3 scatter_custom_fusion
  189.4 4.4 reshape.115
  193.8 134.2 %all_to_all.15 = bf16[128,2,4096]{2,1,0:T(2,128)(2,1)} all-to-all(bf16[128,2,4096]{2,1,0:T(2,128)(2,1)} %reshape.115), channel_id=1, replica_groups=mesh['grp'=2,'sp'=32,'tp'=4] {'sp','tp'}, dimensions={0} | all-to-all | bytes 4194304 | tf_op jit(solution)/shard_map/all_to_all | solution.py:173
  328.0 4.1 reshape.116
  332.1 2.9 fusion.3
  335.0 5.9 %convolution_convert_fusion = bf16[256,4096]{1,0:T(8,128)(2,1)} fusion(bf16[1,256,4096]{2,1,0:T(8,128)(2,1)S(1)} %copy-done, bf16[256,4096]{1,0:T(8,128)(2,1)} %reshape.116, bf16[1,4096,256]{2,1,0:T(8,128)(2,1)} %param.30, f32[256,256]{1,0:T(8,128)S(1)} %fusion.3), kind=kOutput, calls=%fused_computation.2 | convolution fusion | flops 1075183616 | bytes 8650752 | tf_op jit(solution)/shard_map/dot_general | solution.py:125
  341.0 4.4 reshape.117
  345.4 10.2 %all-to-all-start.2 = ((bf16[128,2,4096]{2,1,0:T(2,128)(2,1)}), bf16[128,2,4096]{2,1,0:T(2,128)(2,1)}, u32[]{:S(2)}, u32[]{:S(2)}) async-start(bf16[128,2,4096]{2,1,0:T(2,128)(2,1)} %reshape.117), calls=%async_computation.2 | async-start | bytes 4194304 | tf_op jit(solution)/shard_map/all_to_all | solution.py:183
  355.8 97.7 %all-to-all-done.2 = bf16[128,2,4096]{2,1,0:T(2,128)(2,1)} async-done(((bf16[128,2,4096]{2,1,0:T(2,128)(2,1)}), bf16[128,2,4096]{2,1,0:T(2,128)(2,1)}, u32[]{:S(2)}, u32[]{:S(2)}) %all-to-all-start.2) | async-done | bytes 2097184 | tf_op jit(solution)/shard_map/all_to_all | solution.py:183
  453.5 4.1 reshape.118
  457.7 5.0 %gather_fusion = bf16[128,4096]{1,0:T(8,128)(2,1)} fusion(bf16[256,4096]{1,0:T(8,128)(2,1)} %reshape.118, s32[1024]{0:T(1024)S(1)} %pad_clamp_fusion), kind=kCustom, calls=%fused_computation | custom fusion | bytes 2097664 | tf_op jit(solution)/shard_map/gather | solution.py:184
  462.7 3.4 reshape.119
  466.1 4.8 multiply_reduce_fusion
  471.2 0.3 multiply_reduce_fusion.1
  471.6 1.1 add_convert_fusion
  (42 shorter events, 2.5 us)
Async XLA Ops:
  6.5 328.5 %copy-start = (bf16[1,256,4096]{2,1,0:T(8,128)(2,1)S(1)}, bf16[1,256,4096]{2,1,0:T(8,128)(2,1)}, u32[]{:S(2)}) copy-start(bf16[1,256,4096]{2,1,0:T(8,128)(2,1)} %param.31) | copy-start | bytes 6291460
  6.6 127.9 %all-gather.2.cloned.1.call-start = ((), (), s32[]{:S(2)}) async-start(), calls=%async_computation.3 | async-start | bytes 17301504 | tf_op jit(solution)/shard_map/all_gather | solution.py:153
  13.6 0.8 copy-start.2
  146.8 4.8 %copy-start.7 = (s32[64,2]{0,1:T(2,128)S(1)}, s32[64,2]{0,1:T(2,128)}, u32[]{:S(2)}) copy-start(s32[64,2]{0,1:T(2,128)} %param.28) | copy-start | bytes 1540
  146.8 30.8 %all-to-all-start = ((bf16[4,64,4096]{2,1,0:T(8,128)(2,1)}), bf16[4,64,4096]{2,1,0:T(8,128)(2,1)}, u32[]{:S(2)}, u32[]{:S(2)}) async-start(bf16[4,64,4096]{2,1,0:T(8,128)(2,1)} %bitcast.27), calls=%async_computation | async-start | bytes 4194304 | tf_op jit(solution)/shard_map/all_to_all | solution.py:102
  151.7 28.0 %copy-start.1 = (bf16[64,4096]{1,0:T(8,128)(2,1)S(1)}, bf16[64,4096]{1,0:T(8,128)(2,1)}, u32[]{:S(2)}) copy-start(bf16[64,4096]{1,0:T(8,128)(2,1)} %param.20) | copy-start | bytes 1572868
  179.7 0.7 copy-start.3
  179.7 0.7 copy-start.4
  345.4 10.2 %copy-start.8 = (f32[64,2]{0,1:T(2,128)S(1)}, f32[64,2]{0,1:T(2,128)}, u32[]{:S(2)}) copy-start(f32[64,2]{0,1:T(2,128)} %param.27) | copy-start | bytes 1540
  345.4 10.3 %copy-start.9 = (f32[64]{0:T(128)S(1)}, f32[64]{0:T(128)}, u32[]{:S(2)}) copy-start(f32[64]{0:T(128)} %param.26) | copy-start | bytes 772
  345.4 108.1 %all-to-all-start.2 = ((bf16[128,2,4096]{2,1,0:T(2,128)(2,1)}), bf16[128,2,4096]{2,1,0:T(2,128)(2,1)}, u32[]{:S(2)}, u32[]{:S(2)}) async-start(bf16[128,2,4096]{2,1,0:T(2,128)(2,1)} %reshape.117), calls=%async_computation.2 | async-start | bytes 4194304 | tf_op jit(solution)/shard_map/all_to_all | solution.py:183
  470.9 0.7 copy-start.5
  470.9 0.7 copy-start.6
Sparse Core Ops, SparseCore 0:
  14.6 119.8 all-gather.1
